TPU v7x, 32 devices: a whole 2x2x4 slice. The times are simulated.
32 devices in a mesh: grp: 2 (over y), sp: 4 (over z), tp: 4 (over x, core).
Axes of the slice: x: 2, y: 2, z: 4, core: 2. Of those that a mesh axis runs over, the one named last changes fastest.
Arguments:
- tokens: bfloat16 [2048, 4096], P(('grp', 'sp')), parts along dimension 0, may hold values from -6 to 6
- norm_gain: bfloat16 [2, 4096], replicated, may hold values from 0.099609375 to 1.8984375
- w_query: bfloat16 [2, 4096, 2048], P(None, 'sp', 'tp'), may hold values from -0.09375 to 0.09375
- w_key: bfloat16 [2, 4096, 2048], P(None, 'sp', 'tp'), may hold values from -0.09375 to 0.09375
- w_value: bfloat16 [2, 4096, 2048], P(None, 'sp', 'tp'), may hold values from -0.09375 to 0.09375
- w_out: bfloat16 [2, 2048, 4096], P(None, 'tp', 'sp'), may hold values from -0.125 to 0.125
- offset_bias: float32 [2, 16, 15, 31], P(None, 'tp'), may hold values from -4 to 300
Outputs:
- mixed: bfloat16 [2048, 4096], P(('grp', 'sp')), parts along dimension 0
There are 2 independent parts, one for each index of `grp`. A program takes and returns all parts, laid end to end along the dimension named above; an argument that names none is the same for every part. Nothing has to cross between parts.
All inputs are finite; a program needn't handle non-finite values.
Results may differ from a plain program's by a relative error of at most 0.013.
Values may be sent and summed in bfloat16 or wider, within the bound.
No kernel may reach another device: no remote copies, remote signals or barrier semaphores. Data moves between devices by JAX's collectives and lax.ppermute only.
A program may use at most 128 MiB of HBM per device.

v0:
```python
import jax
import jax.numpy as jnp
from jax import lax
from jax.sharding import PartitionSpec as P

HD = 128
GRID_W = 64
KR = 8
KC = 16
LAYERS = 2
norm_eps = 1e-06


def with_halo(block, sides, width):
    for axis, dim in sides:
        count = lax.axis_size(axis)
        forward = [(i, i + 1) for i in range(count - 1)]
        backward = [(target, source) for source, target in forward]
        low = lax.ppermute(
            lax.slice_in_dim(block, block.shape[dim] - width, None, axis=dim), axis, forward
        )
        high = lax.ppermute(lax.slice_in_dim(block, 0, width, axis=dim), axis, backward)
        block = jnp.concatenate([low, block, high], axis=dim)
    return block


def rms_rows(values, gain):
    wide = values.astype(jnp.float32)
    scaled = wide * lax.rsqrt(jnp.mean(wide * wide, axis=-1, keepdims=True) + norm_eps)
    return (scaled * gain.astype(jnp.float32)).astype(jnp.bfloat16)


def on_device(tokens, norm_gain, w_query, w_key, w_value, w_out, offset_bias):
    sp_count = lax.axis_size("sp")
    sp_index = lax.axis_index("sp")
    tok_rows = tokens.shape[0]
    local_rows = tok_rows // GRID_W
    grid_rows = local_rows * sp_count
    heads_here = offset_bias.shape[1]
    head_width = heads_here * HD
    reach = KR // 2
    scale = HD ** (-0.5)
    columns = jnp.arange(GRID_W, dtype=jnp.int32)
    col_first = jnp.clip(columns - KC // 2, 0, GRID_W - KC)
    col_inside = (columns[None, :] >= col_first[:, None]) & (
        columns[None, :] < col_first[:, None] + KC
    )
    col_offset = jnp.clip(columns[None, :] - columns[:, None], 1 - KC, KC - 1) + KC - 1
    col_onehot = (
        jnp.arange(2 * KC - 1, dtype=jnp.int32)[:, None, None] == col_offset[None, :, :]
    ).astype(jnp.float32)
    first_row = sp_index * local_rows
    own_rows = first_row + jnp.arange(local_rows, dtype=jnp.int32)
    row_first = jnp.clip(own_rows - reach, 0, grid_rows - KR)
    band_start = row_first - first_row + reach
    row_offset = (
        row_first[:, None] + jnp.arange(KR, dtype=jnp.int32)[None, :] - own_rows[:, None] + KR - 1
    )
    row_onehot = (
        row_offset[:, :, None] == jnp.arange(2 * KR - 1, dtype=jnp.int32)[None, None, :]
    ).astype(jnp.float32)
    every_query, every_key, every_value, every_out = (
        lax.all_gather(w_query, "sp", axis=1, tiled=True),
        lax.all_gather(w_key, "sp", axis=1, tiled=True),
        lax.all_gather(w_value, "sp", axis=1, tiled=True),
        lax.all_gather(w_out, "sp", axis=2, tiled=True),
    )
    residual = tokens
    for layer_index in range(LAYERS):
        normed = rms_rows(residual, norm_gain[layer_index])
        queries = jnp.dot(normed, every_query[layer_index], preferred_element_type=jnp.float32)
        keys = jnp.dot(normed, every_key[layer_index], preferred_element_type=jnp.float32)
        values = jnp.dot(normed, every_value[layer_index], preferred_element_type=jnp.float32)
        out_weight = every_out[layer_index]
        queries = queries.astype(jnp.bfloat16).reshape(local_rows, GRID_W, heads_here, HD)
        key_values = jnp.concatenate(
            [keys.astype(jnp.bfloat16), values.astype(jnp.bfloat16)], axis=1
        )
        key_values = key_values.reshape(local_rows, GRID_W, 2 * head_width)
        padded = with_halo(key_values, (("sp", 0),), reach)
        bands = jax.vmap(lambda band_begin: lax.dynamic_slice_in_dim(padded, band_begin, KR, 0))(
            band_start
        )
        band_keys = bands[..., :head_width].reshape(local_rows, KR, GRID_W, heads_here, HD)
        band_values = bands[..., head_width:].reshape(local_rows, KR, GRID_W, heads_here, HD)
        col_bias = jnp.einsum(
            "hro,oqk->hrqk", offset_bias[layer_index], col_onehot, precision=lax.Precision.HIGHEST
        )
        full_bias = jnp.einsum(
            "ijr,hrqk->hiqjk", row_onehot, col_bias, precision=lax.Precision.HIGHEST
        )
        scores = jnp.einsum(
            "iqhd,ijkhd->hiqjk", queries, band_keys, preferred_element_type=jnp.float32
        )
        scores = scores * scale + full_bias
        scores = jnp.where(col_inside[None, None, :, None, :], scores, -jnp.inf)
        flattened = scores.reshape(heads_here, local_rows, GRID_W, KR * GRID_W)
        weights = jax.nn.softmax(flattened, axis=-1).astype(jnp.bfloat16)
        weights = weights.reshape(heads_here, local_rows, GRID_W, KR, GRID_W)
        attended = jnp.einsum(
            "hiqjk,ijkhd->iqhd", weights, band_values, preferred_element_type=jnp.float32
        )
        attended = attended.astype(jnp.bfloat16).reshape(tok_rows, head_width)
        branch = lax.psum(
            jnp.dot(attended, out_weight, preferred_element_type=jnp.float32).astype(jnp.bfloat16),
            "tp",
        ).astype(jnp.float32)
        residual = (residual.astype(jnp.float32) + branch).astype(jnp.bfloat16)
    return residual


def solution(mesh):
    return jax.shard_map(
        on_device,
        mesh=mesh,
        in_specs=(
            P(("grp", "sp"), None),
            P(),
            P(None, "sp", "tp"),
            P(None, "sp", "tp"),
            P(None, "sp", "tp"),
            P(None, "tp", "sp"),
            P(None, "tp", None, None),
        ),
        out_specs=P(("grp", "sp"), None),
        check_vma=False,
    )
```

profile of v0, /device:TPU:0, one launch (start us, length us, event | category | flops | bytes accessed | tf_op | source)
XLA Modules:
  0.0 783.5 jit_solution(1764364375646308337)
XLA Ops:
  6.5 0.7 all-gather.5.cloned.1.call-update
  7.3 0.7 all-gather.7.cloned.1.call-update
  8.1 0.7 all-gather.9.cloned.1.call-update
  8.8 0.5 all-gather.11.cloned.1.call-update
  9.6 1.0 fusion.73
  10.7 3.8 fusion.30
  14.5 6.0 copy.16
  20.5 0.5 fusion
  21.1 140.2 %all-gather.5.cloned.1.call-done = bf16[2,4096,512]{2,1,0:T(8,128)(2,1)} async-done(((bf16[2,1024,512]{2,1,0:T(8,128)(2,1)}), bf16[2,4096,512]{2,1,0:T(8,128)(2,1)}) %all-gather.5.cloned.1.call-update) | async-done | bytes 8388624 | tf_op jit(solution)/shard_map/all_gather | solution.py:64
  161.3 3.5 fusion.54
  164.7 145.9 %all-gather.7.cloned.1.call-done = bf16[2,4096,512]{2,1,0:T(8,128)(2,1)} async-done(((bf16[2,1024,512]{2,1,0:T(8,128)(2,1)}), bf16[2,4096,512]{2,1,0:T(8,128)(2,1)}) %all-gather.7.cloned.1.call-update) | async-done | bytes 8388624 | tf_op jit(solution)/shard_map/all_gather | solution.py:65
  310.7 3.5 fusion.55
  314.2 2.1 collective-permute-start
  316.3 1.5 collective-permute-start.1
  317.8 149.6 %all-gather.9.cloned.1.call-done = bf16[2,4096,512]{2,1,0:T(8,128)(2,1)} async-done(((bf16[2,1024,512]{2,1,0:T(8,128)(2,1)}), bf16[2,4096,512]{2,1,0:T(8,128)(2,1)}) %all-gather.9.cloned.1.call-update) | async-done | bytes 8388624 | tf_op jit(solution)/shard_map/all_gather | solution.py:63
  467.4 3.5 fusion.56
  471.0 2.5 pad_maximum_fusion
  473.5 4.4 gather_fusion
  477.9 3.5 slice_bitcast_fusion.19
  481.4 0.6 copy-done.2
  482.0 1.0 fusion.93
  483.0 0.7 fusion.16
  483.7 1.0 fusion.60
  484.9 132.0 %all-gather.11.cloned.1.call-done = bf16[2,512,4096]{2,1,0:T(8,128)(2,1)} async-done(((bf16[2,512,1024]{2,1,0:T(8,128)(2,1)}), bf16[2,512,4096]{2,1,0:T(8,128)(2,1)}) %all-gather.11.cloned.1.call-update) | async-done | bytes 8388624 | tf_op jit(solution)/shard_map/all_gather | solution.py:66
  616.9 4.8 convolution_convert_fusion.1
  621.8 2.4 fusion.71
  624.2 47.2 %all-reduce.4.cloned.1.call-done = bf16[256,4096]{1,0:T(8,128)(2,1)} async-done(((bf16[256,4096]{1,0:T(8,128)(2,1)}), bf16[256,4096]{1,0:T(8,128)(2,1)}) %all-reduce.4.cloned.1.call-update) | async-done | bytes 2097168 | tf_op jit(solution)/shard_map/psum | solution.py:104
  671.5 2.5 fusion.4
  674.0 1.0 fusion.6
  675.0 4.5 fusion.57
  679.5 1.2 fusion.58
  680.8 3.4 collective-permute-start.2
  684.3 1.5 collective-permute-start.3
  685.8 3.9 fusion.28
  689.7 5.8 copy.22
  695.4 4.8 fusion.59
  700.2 1.0 reshape.189
  701.3 2.4 pad_maximum_fusion.1
  703.6 4.2 gather_fusion.1
  707.8 3.1 slice_bitcast_fusion.17
  710.9 0.3 copy-done.3
  711.3 1.0 fusion.94
  712.3 0.7 fusion.17
  713.0 1.0 fusion.65
  714.5 1.5 slice-done.1
  715.9 2.6 convolution_convert_fusion
  718.6 53.4 %all-reduce.6.cloned.1.call-done = bf16[256,4096]{1,0:T(8,128)(2,1)} async-done(((bf16[256,4096]{1,0:T(8,128)(2,1)}), bf16[256,4096]{1,0:T(8,128)(2,1)}) %all-reduce.6.cloned.1.call-update) | async-done | bytes 2097168 | tf_op jit(solution)/shard_map/psum | solution.py:104
  771.9 4.7 fusion.7
  (51 shorter events, 1.5 us)
Async XLA Ops:
  6.5 2.9 copy-start.7
  6.5 154.7 %all-gather.5.cloned.1.call-start = ((), (), s32[]{:S(2)}) async-start(), calls=%async_computation | async-start | bytes 10485760 | tf_op jit(solution)/shard_map/all_gather | solution.py:64
  7.3 303.4 %all-gather.7.cloned.1.call-start = ((), (), s32[]{:S(2)}) async-start(), calls=%async_computation.1 | async-start | bytes 10485760 | tf_op jit(solution)/shard_map/all_gather | solution.py:65
  8.0 459.4 %all-gather.9.cloned.1.call-start = ((), (), s32[]{:S(2)}) async-start(), calls=%async_computation.2 | async-start | bytes 10485760 | tf_op jit(solution)/shard_map/all_gather | solution.py:63
  8.7 608.2 %all-gather.11.cloned.1.call-start = ((), (), s32[]{:S(2)}) async-start(), calls=%async_computation.3 | async-start | bytes 10485760 | tf_op jit(solution)/shard_map/all_gather | solution.py:66
  9.3 662.1 %all-reduce.4.cloned.1.call-start = ((), (), s32[]{:S(2)}) async-start(), calls=%async_computation.4 | async-start | bytes 4194304 | tf_op jit(solution)/shard_map/psum | solution.py:104
  14.5 6.0 copy-start
  14.5 6.6 copy-start.6
  314.2 156.7 %collective-permute-start = (bf16[4,64,1024]{2,1,0:T(8,128)(2,1)S(1)}, bf16[4,64,1024]{2,1,0:T(8,128)(2,1)}, u32[]{:S(2)}, u32[]{:S(2)}) collective-permute-start(bf16[4,64,1024]{2,1,0:T(8,128)(2,1)S(1)} %bitcast.150), channel_id=1, source_target_pairs={{0,4},{4,8},{8,12},{1,5},{5,9},{9,13},{2,6},{6,10},{10,14},{3,7},{... | collective-permute-start | bytes 1572872 | tf_op jit(solution)/shard_map/ppermute | solution.py:19
  316.3 154.6 %collective-permute-start.1 = (bf16[4,64,1024]{2,1,0:T(8,128)(2,1)S(1)}, bf16[4,64,1024]{2,1,0:T(8,128)(2,1)}, u32[]{:S(2)}, u32[]{:S(2)}) collective-permute-start(bf16[4,64,1024]{2,1,0:T(8,128)(2,1)S(1)} %bitcast.151), channel_id=1, source_target_pairs={{4,0},{8,4},{12,8},{5,1},{9,5},{13,9},{6,2},{10,6},{14,10},{7,3},{... | collective-permute-start | bytes 1572872 | tf_op jit(solution)/shard_map/ppermute | solution.py:22
  477.9 4.1 copy-start.2
  621.7 150.2 %all-reduce.6.cloned.1.call-start = ((), (), s32[]{:S(2)}) async-start(), calls=%async_computation.5 | async-start | bytes 4194304 | tf_op jit(solution)/shard_map/psum | solution.py:104
  671.5 2.5 copy-start.1
  674.0 5.5 slice-start.2
  674.9 4.5 copy-start.5
  675.0 4.6 slice-start.3
  679.5 6.3 copy-start.4
  680.8 20.4 %collective-permute-start.2 = (bf16[4,64,1024]{2,1,0:T(8,128)(2,1)S(1)}, bf16[4,64,1024]{2,1,0:T(8,128)(2,1)S(1)}, u32[]{:S(2)}, u32[]{:S(2)}) collective-permute-start(bf16[4,64,1024]{2,1,0:T(8,128)(2,1)S(1)} %bitcast.147), channel_id=1, source_target_pairs={{0,4},{4,8},{8,12},{1,5},{5,9},{9,13},{2,6},{6,10},{10,14},{3,7},{... | collective-permute-start | bytes 1572872 | tf_op jit(solution)/shard_map/ppermute | solution.py:19
  684.3 17.0 %collective-permute-start.3 = (bf16[4,64,1024]{2,1,0:T(8,128)(2,1)S(1)}, bf16[4,64,1024]{2,1,0:T(8,128)(2,1)}, u32[]{:S(2)}, u32[]{:S(2)}) collective-permute-start(bf16[4,64,1024]{2,1,0:T(8,128)(2,1)S(1)} %bitcast.148), channel_id=1, source_target_pairs={{4,0},{8,4},{12,8},{5,1},{9,5},{13,9},{6,2},{10,6},{14,10},{7,3},{... | collective-permute-start | bytes 1572872 | tf_op jit(solution)/shard_map/ppermute | solution.py:22
  707.8 3.4 copy-start.3
  712.3 2.2 slice-start
  713.0 2.9 slice-start.1
Sparse Core Ops, SparseCore 0:
  8.9 152.3 all-gather.4
  162.8 147.7 all-gather.6
  312.2 155.1 all-gather.8
  468.8 148.0 all-gather.10
  621.9 49.5 all-reduce.3
  718.7 53.1 all-reduce.5
where the time goes:
time: 784 us; the launch traced here: 783 us
  waiting for transfers between devices  671 us (86%)
  matrix products  43.4 us (6%)
  local copies, waits for them, and re-layouts  31.2 us (4%)
  other arithmetic  15.4 us (2%)
  between operations  13.8 us (2%)
  starting transfers between devices  8.71 us (1%)
    all_gather x1, waiting for transfers between devices, on_device(): lax.all_gather(w_query, 'sp', axis=1, tiled=True)  150 us
    all_gather x1, waiting for transfers between devices, on_device(): lax.all_gather(w_value, 'sp', axis=1, tiled=True)  146 us
    all_gather x1, waiting for transfers between devices, on_device(): lax.all_gather(w_key, 'sp', axis=1, tiled=True)  140 us
    all_gather x1, waiting for transfers between devices, on_device(): lax.all_gather(w_out, 'sp', axis=2, tiled=True)  132 us
    psum x2, waiting for transfers between devices, on_device(): lax.psum(jnp.dot(attended, out_weight, preferred_element_type=jnp.float32...  101 us
  transfers between devices with their start and end apart: 10, of which 6 were waited for; matrix products, arithmetic and copies ran while one was open for 7% of the time, Pallas kernels for 0%

commit v1 on v0

--- a/solution.py
+++ b/solution.py
@@ -9,6 +9,11 @@
 KC = 16
 LAYERS = 2
 norm_eps = 1e-06
+
+
+def gathered_along(array, name, along):
+    tiles = lax.all_gather(array, name)
+    return jnp.concatenate(tiles, axis=along)
 
 
 def with_halo(block, sides, width):
@@ -61,7 +66,7 @@
     ).astype(jnp.float32)
     every_query, every_key, every_value, every_out = (
         lax.all_gather(w_query, "sp", axis=1, tiled=True),
-        lax.all_gather(w_key, "sp", axis=1, tiled=True),
+        gathered_along(w_key, "sp", 1),
         lax.all_gather(w_value, "sp", axis=1, tiled=True),
         lax.all_gather(w_out, "sp", axis=2, tiled=True),
     )

time: 784 us -> 785 us (level)
  no operation moved by 1% of the time
where the time goes in v1:
time: 785 us; the launch traced here: 784 us
  waiting for transfers between devices  668 us (85%)
  matrix products  40.9 us (5%)
  local copies, waits for them, and re-layouts  38.7 us (5%)
  other arithmetic  15.1 us (2%)
  between operations  13.8 us (2%)
  starting transfers between devices  7.93 us (1%)
    all_gather x1, waiting for transfers between devices, on_device(): lax.all_gather(w_query, 'sp', axis=1, tiled=True)  150 us
    all_gather x1, waiting for transfers between devices, on_device(): lax.all_gather(w_value, 'sp', axis=1, tiled=True)  143 us
    all_gather x1, waiting for transfers between devices, gathered_along(): tiles = lax.all_gather(array, name)  140 us
    all_gather x1, waiting for transfers between devices, on_device(): lax.all_gather(w_out, 'sp', axis=2, tiled=True)  131 us
    psum x2, waiting for transfers between devices, on_device(): lax.psum(jnp.dot(attended, out_weight, preferred_element_type=jnp.float32...  101 us
  transfers between devices with their start and end apart: 10, of which 6 were waited for; matrix products, arithmetic and copies ran while one was open for 7% of the time, Pallas kernels for 0%

profile of v1, /device:TPU:0, one launch (start us, length us, event | category | flops | bytes accessed | tf_op | source)
XLA Modules:
  0.0 784.2 jit_solution(17233687865404392574)
XLA Ops:
  6.5 0.7 all-gather.12.cloned.1.call-update
  7.3 0.7 all-gather.6.cloned.1.call-update
  8.1 0.7 all-gather.8.cloned.1.call-update
  8.8 0.5 all-gather.10.cloned.1.call-update
  9.5 1.0 fusion.69
  10.5 3.9 fusion.28
  14.4 6.0 copy.29
  21.0 140.3 %all-gather.12.cloned.1.call-done = bf16[8,1024,512]{2,1,0:T(8,128)(2,1)} async-done(((bf16[2,1024,512]{2,1,0:T(8,128)(2,1)}), bf16[8,1024,512]{2,1,0:T(8,128)(2,1)}) %all-gather.12.cloned.1.call-update) | async-done | bytes 8388624 | tf_op jit(solution)/shard_map/all_gather | solution.py:15
  161.3 5.1 fusion.89
  166.4 1.3 convolution_convert_fusion.3
  167.7 142.9 %all-gather.6.cloned.1.call-done = bf16[2,4096,512]{2,1,0:T(8,128)(2,1)} async-done(((bf16[2,1024,512]{2,1,0:T(8,128)(2,1)}), bf16[2,4096,512]{2,1,0:T(8,128)(2,1)}) %all-gather.6.cloned.1.call-update) | async-done | bytes 8388624 | tf_op jit(solution)/shard_map/all_gather | solution.py:70
  310.7 3.5 fusion.52
  314.2 1.3 collective-permute-start
  315.5 1.5 collective-permute-start.1
  317.0 150.4 %all-gather.8.cloned.1.call-done = bf16[2,4096,512]{2,1,0:T(8,128)(2,1)} async-done(((bf16[2,1024,512]{2,1,0:T(8,128)(2,1)}), bf16[2,4096,512]{2,1,0:T(8,128)(2,1)}) %all-gather.8.cloned.1.call-update) | async-done | bytes 8388624 | tf_op jit(solution)/shard_map/all_gather | solution.py:68
  467.4 4.2 fusion.53
  471.6 1.0 reshape.193
  472.6 2.4 pad_maximum_fusion
  475.0 4.4 gather_fusion
  479.5 3.3 slice_bitcast_fusion.15
  483.2 1.0 fusion.91
  484.2 0.7 fusion.14
  484.9 1.0 fusion.56
  486.1 130.8 %all-gather.10.cloned.1.call-done = bf16[2,512,4096]{2,1,0:T(8,128)(2,1)} async-done(((bf16[2,512,1024]{2,1,0:T(8,128)(2,1)}), bf16[2,512,4096]{2,1,0:T(8,128)(2,1)}) %all-gather.10.cloned.1.call-update) | async-done | bytes 8388624 | tf_op jit(solution)/shard_map/all_gather | solution.py:71
  616.9 4.8 convolution_convert_fusion.1
  621.8 2.3 fusion.67
  624.1 47.4 %all-reduce.4.cloned.1.call-done = bf16[256,4096]{1,0:T(8,128)(2,1)} async-done(((bf16[256,4096]{1,0:T(8,128)(2,1)}), bf16[256,4096]{1,0:T(8,128)(2,1)}) %all-reduce.4.cloned.1.call-update) | async-done | bytes 2097168 | tf_op jit(solution)/shard_map/psum | solution.py:109
  671.4 2.5 fusion.4
  674.0 1.0 fusion.6
  675.0 1.8 copy-done.5
  676.8 1.2 convolution_convert_fusion.2
  678.0 3.6 fusion.54
  681.7 3.4 collective-permute-start.2
  685.1 1.5 collective-permute-start.3
  686.7 3.8 fusion.26
  690.5 5.8 copy.36
  696.3 4.8 fusion.55
  701.0 1.0 reshape.198
  702.1 2.4 pad_maximum_fusion.1
  704.4 4.2 gather_fusion.1
  708.6 3.1 slice_bitcast_fusion.13
  712.1 1.0 fusion.92
  713.1 0.7 fusion.15
  713.8 1.0 fusion.61
  715.3 1.5 slice-done.1
  716.7 2.6 convolution_convert_fusion
  719.4 53.3 %all-reduce.6.cloned.1.call-done = bf16[256,4096]{1,0:T(8,128)(2,1)} async-done(((bf16[256,4096]{1,0:T(8,128)(2,1)}), bf16[256,4096]{1,0:T(8,128)(2,1)}) %all-reduce.6.cloned.1.call-update) | async-done | bytes 2097168 | tf_op jit(solution)/shard_map/psum | solution.py:109
  772.7 4.7 fusion.7
  (48 shorter events, 2.4 us)
Async XLA Ops:
  6.5 2.9 copy-start.8
  6.5 154.7 %all-gather.12.cloned.1.call-start = ((), (), s32[]{:S(2)}) async-start(), calls=%async_computation.5 | async-start | bytes 10485760 | tf_op jit(solution)/shard_map/all_gather | solution.py:15
  7.3 303.4 %all-gather.6.cloned.1.call-start = ((), (), s32[]{:S(2)}) async-start(), calls=%async_computation | async-start | bytes 10485760 | tf_op jit(solution)/shard_map/all_gather | solution.py:70
  8.0 459.4 %all-gather.8.cloned.1.call-start = ((), (), s32[]{:S(2)}) async-start(), calls=%async_computation.1 | async-start | bytes 10485760 | tf_op jit(solution)/shard_map/all_gather | solution.py:68
  8.7 608.2 %all-gather.10.cloned.1.call-start = ((), (), s32[]{:S(2)}) async-start(), calls=%async_computation.2 | async-start | bytes 10485760 | tf_op jit(solution)/shard_map/all_gather | solution.py:71
  9.3 662.1 %all-reduce.4.cloned.1.call-start = ((), (), s32[]{:S(2)}) async-start(), calls=%async_computation.3 | async-start | bytes 4194304 | tf_op jit(solution)/shard_map/psum | solution.py:109
  14.4 6.0 copy-start
  14.4 6.6 copy-start.7
  314.2 158.4 %collective-permute-start = (bf16[4,64,1024]{2,1,0:T(8,128)(2,1)S(1)}, bf16[4,64,1024]{2,1,0:T(8,128)(2,1)S(1)}, u32[]{:S(2)}, u32[]{:S(2)}) collective-permute-start(bf16[4,64,1024]{2,1,0:T(8,128)(2,1)S(1)} %bitcast.158), channel_id=1, source_target_pairs={{0,4},{4,8},{8,12},{1,5},{5,9},{9,13},{2,6},{6,10},{10,14},{3,7},{... | collective-permute-start | bytes 1572872 | tf_op jit(solution)/shard_map/ppermute | solution.py:24
  315.5 157.1 %collective-permute-start.1 = (bf16[4,64,1024]{2,1,0:T(8,128)(2,1)S(1)}, bf16[4,64,1024]{2,1,0:T(8,128)(2,1)}, u32[]{:S(2)}, u32[]{:S(2)}) collective-permute-start(bf16[4,64,1024]{2,1,0:T(8,128)(2,1)S(1)} %bitcast.159), channel_id=1, source_target_pairs={{4,0},{8,4},{12,8},{5,1},{9,5},{13,9},{6,2},{10,6},{14,10},{7,3},{... | collective-permute-start | bytes 1572872 | tf_op jit(solution)/shard_map/ppermute | solution.py:27
  479.5 3.7 copy-start.2
  621.7 151.0 %all-reduce.6.cloned.1.call-start = ((), (), s32[]{:S(2)}) async-start(), calls=%async_computation.4 | async-start | bytes 4194304 | tf_op jit(solution)/shard_map/psum | solution.py:109
  671.4 2.5 copy-start.1
  673.9 2.8 copy-start.5
  674.9 6.7 copy-start.6
  678.0 8.6 %copy-start.4 = (f32[64,64,4,15]{1,3,0,2:T(8,128)S(1)}, f32[64,64,4,15]{1,3,0,2:T(8,128)}, u32[]{:S(2)}) copy-start(f32[64,64,4,15]{1,3,0,2:T(8,128)} %fusion.67) | copy-start | bytes 2949124
  681.7 20.4 %collective-permute-start.2 = (bf16[4,64,1024]{2,1,0:T(8,128)(2,1)S(1)}, bf16[4,64,1024]{2,1,0:T(8,128)(2,1)S(1)}, u32[]{:S(2)}, u32[]{:S(2)}) collective-permute-start(bf16[4,64,1024]{2,1,0:T(8,128)(2,1)S(1)} %bitcast.155), channel_id=1, source_target_pairs={{0,4},{4,8},{8,12},{1,5},{5,9},{9,13},{2,6},{6,10},{10,14},{3,7},{... | collective-permute-start | bytes 1572872 | tf_op jit(solution)/shard_map/ppermute | solution.py:24
  685.1 17.0 %collective-permute-start.3 = (bf16[4,64,1024]{2,1,0:T(8,128)(2,1)S(1)}, bf16[4,64,1024]{2,1,0:T(8,128)(2,1)}, u32[]{:S(2)}, u32[]{:S(2)}) collective-permute-start(bf16[4,64,1024]{2,1,0:T(8,128)(2,1)S(1)} %bitcast.156), channel_id=1, source_target_pairs={{4,0},{8,4},{12,8},{5,1},{9,5},{13,9},{6,2},{10,6},{14,10},{7,3},{... | collective-permute-start | bytes 1572872 | tf_op jit(solution)/shard_map/ppermute | solution.py:27
  708.6 3.4 copy-start.3
  713.1 2.2 slice-start
  713.8 2.9 slice-start.1
Sparse Core Ops, SparseCore 0:
  8.9 152.3 all-gather.11
  162.8 147.7 all-gather.5
  312.2 155.1 all-gather.7
  468.8 148.0 all-gather.9
  621.8 49.5 all-reduce.3
  719.5 53.1 all-reduce.5
